TPU v7x, 512 devices: a whole 4x8x8 slice. The times are simulated.
512 devices in a mesh: ep: 32 (over z, x), tp: 16 (over y, core).
Axes of the slice: x: 4, y: 8, z: 8, core: 2. Of those that a mesh axis runs over, the one named last changes fastest.
Arguments:
- conv_value: bfloat16 [16384, 2048], P('ep', 'tp'), may hold values from -6 to 6
- conv_gate: bfloat16 [16384, 2048], P('ep', 'tp'), may hold values from -9 to 9
- conv_taps: float32 [31, 2048], P(None, 'tp'), may hold values from -14 to 14
- norm_gain: float32 [2048], P('tp'), may hold values from 0.1 to 1.9
- norm_shift: float32 [2048], P('tp'), may hold values from -3 to 3
- conv_out_weight: bfloat16 [2048, 2048], P(None, 'tp'), may hold values from -0.125 to 0.125
- moe_input: bfloat16 [4096, 2048], P('ep'), may hold values from -6 to 6
- moe_gain: float32 [2048], replicated, may hold values from 0.1 to 1.9
- routes: int32 [4096, 4], P('ep'), may hold values from 0 to 31, all different within a row; in each aligned block of 128 rows (0 to 127, 128 to 255, ...) at most 32 rows name the same one
- route_weights: float32 [4096, 4], P('ep'), may hold values from 0.25 to 1
- expert_gate: bfloat16 [32, 2048, 4096], P('ep', None, 'tp'), may hold values from -0.125 to 0.125
- expert_up: bfloat16 [32, 2048, 4096], P('ep', None, 'tp'), may hold values from -0.125 to 0.125
- expert_down: bfloat16 [32, 4096, 2048], P('ep', None, 'tp'), may hold values from -0.09375 to 0.09375
- shared_gate: bfloat16 [2048, 512], P(None, 'tp'), may hold values from -0.125 to 0.125
- shared_up: bfloat16 [2048, 512], P(None, 'tp'), may hold values from -0.125 to 0.125
- shared_down: bfloat16 [512, 2048], P(None, 'tp'), may hold values from -0.25 to 0.25
Outputs:
- conv_result: bfloat16 [16384, 2048], P('ep', 'tp')
- moe_result: bfloat16 [4096, 2048], P('ep', 'tp')
Inputs may be any that keep to these rules, and one draw needn't show every extreme that they name: `routes`: in the rows of one device (aligned blocks of 128 rows) no expert is named by more than 32 rows, a bound that some block reaches; each row names 4 different experts.
All inputs are finite; a program needn't handle non-finite values.
Results may differ from a plain program's by a relative error of at most 0.0068.
Values may be sent and summed in bfloat16 or wider, within the bound.
A program may use at most 64 MiB of HBM per device.

v0:
```python
import jax
import jax.numpy as jnp
from jax import lax
from jax.sharding import Mesh
from jax.sharding import PartitionSpec as P

EP = ("ep_0", "ep_1")


def from_behind(value, axis, steps):
    count = lax.axis_size(axis)
    initial, last = (max(0, -steps), min(count, count - steps))
    return lax.ppermute(value, axis, [(source, source + steps) for source in range(initial, last)])


def cut_along(array, dim, peers):
    before, after = (array.shape[:dim], array.shape[dim + 1 :])
    return jnp.moveaxis(array.reshape(*before, peers, -1, *after), dim, 0)


def joined_along(parts, dim):
    lengths = list(parts.shape[1:])
    lengths[dim] *= parts.shape[0]
    return jnp.moveaxis(parts, 0, dim).reshape(lengths)


def exchange_in_order(parts, axes, turns):
    lengths = [lax.axis_size(a) for a in axes]
    parts = parts.reshape(*lengths, *parts.shape[1:])
    for k in turns:
        parts = lax.all_to_all(parts, axes[k], split_axis=k, concat_axis=k, tiled=True)
    return parts.reshape(-1, *parts.shape[len(axes) :])


def stepwise_exchange(array, axes, turns, split_dim, concat_dim):
    parts = cut_along(array, split_dim, lax.axis_size(axes))
    return joined_along(exchange_in_order(parts, axes, turns), concat_dim)


def body(
    conv_value,
    conv_gate,
    conv_taps,
    norm_gain,
    norm_shift,
    conv_out_weight,
    moe_input,
    moe_gain,
    routes,
    route_weights,
    expert_gate,
    expert_up,
    expert_down,
    shared_gate,
    shared_up,
    shared_down,
):
    tap_count = conv_taps.shape[0]
    rows_a = conv_value.shape[0]
    glu_rows = (
        conv_value.astype(jnp.float32) * jax.nn.sigmoid(conv_gate.astype(jnp.float32))
    ).astype(jnp.bfloat16)
    before = from_behind(glu_rows[rows_a - (tap_count - 1) :], EP, 1)
    padded = jnp.concatenate([before, glu_rows], axis=0)
    filtered = jnp.zeros(glu_rows.shape, jnp.float32)
    for offset in range(tap_count):
        filtered = filtered + conv_taps[offset] * padded[offset : offset + rows_a].astype(
            jnp.float32
        )
    row_total, squares = lax.psum(
        (jnp.sum(filtered, axis=1), jnp.sum(filtered * filtered, axis=1)), "tp"
    )
    channels = conv_out_weight.shape[0]
    row_mean = row_total / channels
    row_square = squares / channels
    scaled = (filtered - row_mean[:, None]) * lax.rsqrt(row_square - row_mean * row_mean + 1e-05)[
        :, None
    ]
    conv_hidden = jax.nn.silu(scaled * norm_gain + norm_shift).astype(jnp.bfloat16)
    conv_sum = jnp.dot(
        lax.all_gather(conv_hidden, "tp", axis=1, tiled=True),
        conv_out_weight,
        preferred_element_type=jnp.float32,
    )
    conv_result = conv_sum.astype(jnp.bfloat16)
    inputs = moe_input.astype(jnp.float32)
    normed = (
        inputs * lax.rsqrt(jnp.mean(inputs * inputs, axis=1, keepdims=True) + 1e-06) * moe_gain
    ).astype(jnp.bfloat16)
    rows_b, per_row = routes.shape
    model_width = normed.shape[1]
    groups = lax.axis_size(EP)
    capacity = 2 * rows_b * per_row // groups
    flat_expert = routes.reshape(-1)
    owner_row = jnp.arange(rows_b * per_row, dtype=jnp.int32) // per_row
    expert_hits = (flat_expert[:, None] == jnp.arange(groups, dtype=jnp.int32)[None, :]).astype(
        jnp.int32
    )
    slot_rank = jnp.sum((jnp.cumsum(expert_hits, axis=0) - expert_hits) * expert_hits, axis=1)
    slot_index = flat_expert * capacity + slot_rank
    outgoing = (
        jnp.zeros((groups * capacity, model_width), jnp.bfloat16)
        .at[slot_index]
        .set(normed[owner_row])
    )
    outgoing = outgoing.reshape(groups, capacity, model_width)
    slot_share = capacity // lax.axis_size("tp")
    own_slots = lax.dynamic_slice_in_dim(outgoing, lax.axis_index("tp") * slot_share, slot_share, 1)
    partial_rows = lax.all_to_all(own_slots, EP, split_axis=0, concat_axis=0, tiled=True)
    arrived = lax.all_gather(partial_rows, "tp", axis=1, tiled=True)
    arrived_rows = arrived.reshape(groups * capacity, model_width)
    gate_value = jnp.dot(arrived_rows, expert_gate[0], preferred_element_type=jnp.float32)
    upward = jnp.dot(arrived_rows, expert_up[0], preferred_element_type=jnp.float32)
    expert_hidden = (jax.nn.silu(gate_value) * upward).astype(jnp.bfloat16)
    shared_hidden = (
        jax.nn.silu(jnp.dot(normed, shared_gate, preferred_element_type=jnp.float32))
        * jnp.dot(normed, shared_up, preferred_element_type=jnp.float32)
    ).astype(jnp.bfloat16)
    columns = expert_down.shape[2]
    routed_rows = expert_down[0]
    routed_sum = jnp.dot(
        lax.all_gather(expert_hidden, "tp", axis=1, tiled=True),
        routed_rows,
        preferred_element_type=jnp.float32,
    )
    shared_sum = jnp.dot(
        lax.all_gather(shared_hidden, "tp", axis=1, tiled=True),
        shared_down,
        preferred_element_type=jnp.float32,
    )
    expert_out = routed_sum.astype(jnp.bfloat16).reshape(groups, capacity, columns)
    returned = stepwise_exchange(expert_out, EP, (0, 1), 0, 0).reshape(groups * capacity, columns)
    picked = returned[slot_index].astype(jnp.float32) * route_weights.reshape(-1)[:, None]
    moe_sum = jnp.sum(picked.reshape(rows_b, per_row, columns), axis=1) + shared_sum
    return (conv_result, moe_sum.astype(jnp.bfloat16))


def solution(mesh):
    finer = Mesh(mesh.devices.reshape(8, 4, mesh.shape["tp"]), ("ep_0", "ep_1", "tp"))
    in_specs = (
        P(EP, "tp"),
        P(EP, "tp"),
        P(None, "tp"),
        P("tp"),
        P("tp"),
        P(None, "tp"),
        P(EP, None),
        P(),
        P(EP, None),
        P(EP, None),
        P(EP, None, "tp"),
        P(EP, None, "tp"),
        P(EP, None, "tp"),
        P(None, "tp"),
        P(None, "tp"),
        P(None, "tp"),
    )
    out_specs = (P(EP, "tp"), P(EP, "tp"))
    return jax.shard_map(body, mesh=finer, in_specs=in_specs, out_specs=out_specs, check_vma=False)
```

profile of v0, /device:TPU:1, one launch (start us, length us, event | category | flops | bytes accessed | tf_op | source)
XLA Modules:
  0.0 226.3 jit_solution(18367188397835349781)
XLA Ops:
  8.0 0.8 copy.33
  9.0 1.2 fusion.6
  10.5 1.2 reduce-window.6
  12.1 1.2 fusion.8
  13.3 12.8 %scatter_custom_fusion = bf16[1024,2048]{1,0:T(8,128)(2,1)} fusion(s32[512]{0:T(512)S(1)} %bitcast.118, bf16[128,2048]{1,0:T(8,128)(2,1)S(1)} %fusion.8, s32[1024]{0:T(1024)S(1)} %pad_clamp_fusion.1, bf16[]{:T(256)} %constant.47.clone.1), kind=kCustom, calls=%fused_computation.3 | custom fusion | bytes 4194306 | tf_op jit(solution)/shard_map/scatter | solution.py:104
  26.1 1.5 constant_dynamic-slice_fusion
  27.6 24.8 %all_to_all.15 = bf16[32,2,2048]{2,1,0:T(2,128)(2,1)S(1)} all-to-all(bf16[32,2,2048]{2,1,0:T(2,128)(2,1)S(1)} %constant_dynamic-slice_fusion), channel_id=1, replica_groups=mesh['ep_0'=8,'ep_1'=4,'tp'=16] {'ep_0','ep_1'}, dimensions={0} | all-to-all | bytes 524288 | tf_op jit(solution)/shard_map/all_to_all | solution.py:109
  53.3 42.1 %all-gather.6.cloned.1.call-done = bf16[32,32,2048]{2,0,1:T(8,128)(2,1)} async-done(((bf16[32,2,2048]{2,0,1:T(8,128)(2,1)}), bf16[32,32,2048]{2,0,1:T(8,128)(2,1)}) %all-gather.6.cloned.1.call-update) | async-done | bytes 4194320 | tf_op jit(solution)/shard_map/all_gather | solution.py:110
  95.4 4.5 %copy.37 = bf16[32,32,2048]{2,1,0:T(8,128)(2,1)S(1)} copy(bf16[32,32,2048]{2,0,1:T(8,128)(2,1)} %all-gather.6.cloned.1.call-done) | data formatting | bytes 8388608 | tf_op jit(solution)/shard_map/all_gather | solution.py:110
  99.9 1.3 fusion.11
  101.2 2.1 fusion.3
  103.5 3.1 %collective-permute-start = (bf16[30,128]{1,0:T(8,128)(2,1)S(1)}, bf16[30,128]{1,0:T(8,128)(2,1)S(1)}, u32[]{:S(2)}, u32[]{:S(2)}) collective-permute-start(bf16[30,128]{1,0:T(8,128)(2,1)S(1)} %slice.260), channel_id=1, source_target_pairs={{0,16},{16,32},{32,48},{48,64},{64,80},{80,96},{96,112},{112,128},... | collective-permute-start | bytes 23048 | tf_op jit(solution)/shard_map/ppermute | solution.py:13
  107.4 1.2 fusion.47
  108.6 25.0 %all-reduce = (f32[512]{0:T(512)S(1)}, f32[512]{0:T(512)S(1)}) all-reduce(f32[512]{0:T(512)S(1)} %get-tuple-element.3, f32[512]{0:T(512)S(1)} %get-tuple-element.2), channel_id=1, replica_groups=mesh['ep_0'=8,'ep_1'=4,'tp'=16] {'tp'}, use_global_device_ids=true, to_apply=%region_3.0 | all-reduce | flops 1024 | bytes 8192 | tf_op jit(solution)/shard_map/psum | solution.py:70
  133.7 0.9 multiply_convert_fusion
  134.6 35.8 %all-gather.8.cloned.1.call-done = bf16[1024,4096]{1,0:T(8,128)(2,1)} async-done(((bf16[1024,256]{1,0:T(8,128)(2,1)}), bf16[1024,4096]{1,0:T(8,128)(2,1)}) %all-gather.8.cloned.1.call-update) | async-done | bytes 8388624 | tf_op jit(solution)/shard_map/all_gather | solution.py:122
  170.4 6.7 %convolution_convert_fusion = bf16[1024,128]{1,0:T(8,128)(2,1)} fusion(bf16[1024,4096]{1,0:T(8,128)(2,1)} %all-gather.8.cloned.1.call-done, bf16[1,4096,128]{2,1,0:T(8,128)(2,1)} %param.28), kind=kOutput, calls=%fused_computation.39 | convolution fusion | flops 1073872896 | bytes 9699328 | tf_op jit(solution)/shard_map/dot_general | solution.py:121
  177.1 6.5 %all-to-all-start.1 = ((bf16[8,4,1,32,128]{4,3,1,2,0:T(8,128)(2,1)}), bf16[8,4,1,32,128]{4,3,1,2,0:T(8,128)(2,1)S(1)}, u32[]{:S(2)}, u32[]{:S(2)}) async-start(bf16[8,4,1,32,128]{4,3,1,2,0:T(8,128)(2,1)} %bitcast.41), calls=%async_computation.1 | async-start | bytes 524288 | tf_op jit(solution)/shard_map/all_to_all | solution.py:31
  184.3 16.1 %all_gather.15 = bf16[128,512]{0,1:T(8,128)(2,1)S(1)} all-gather(bf16[128,32]{0,1:T(8,128)(2,1)S(1)} %fusion.5), channel_id=1, replica_groups=mesh['ep_0'=8,'ep_1'=4,'tp'=16] {'tp'}, dimensions={1}, use_global_device_ids=true | all-gather | bytes 139264 | tf_op jit(solution)/shard_map/all_gather | solution.py:127
  201.1 4.1 %all-to-all-start.2 = ((bf16[8,4,1,32,128]{4,3,0,2,1:T(8,128)(2,1)}), bf16[8,4,1,32,128]{4,3,0,2,1:T(8,128)(2,1)S(1)}, u32[]{:S(2)}, u32[]{:S(2)}) async-start(bf16[8,4,1,32,128]{4,3,0,2,1:T(8,128)(2,1)} %copy.39), calls=%async_computation.2 | async-start | bytes 524288 | tf_op jit(solution)/shard_map/all_to_all | solution.py:31
  205.2 9.1 %all-gather.4.cloned.1.call-done = bf16[512,2048]{1,0:T(8,128)(2,1)} async-done(((bf16[512,128]{1,0:T(8,128)(2,1)}), bf16[512,2048]{1,0:T(8,128)(2,1)}) %all-gather.4.cloned.1.call-update) | async-done | bytes 2097168 | tf_op jit(solution)/shard_map/all_gather | solution.py:81
  214.3 3.0 %convolution_convert_fusion.1 = bf16[512,128]{1,0:T(8,128)(2,1)} fusion(bf16[512,2048]{1,0:T(8,128)(2,1)} %all-gather.4.cloned.1.call-done, bf16[2048,128]{1,0:T(8,128)(2,1)S(1)} %copy-done.1), kind=kOutput, calls=%fused_computation.40 | convolution fusion | flops 268500992 | bytes 2752512 | tf_op jit(solution)/shard_map/dot_general | solution.py:80
  217.3 1.3 gather_fusion
  218.9 0.8 fusion.4
  (60 shorter events, 5.1 us)
Async XLA Ops:
  7.2 92.7 %copy-start = (bf16[1,2048,256]{2,1,0:T(8,128)(2,1)S(1)}, bf16[1,2048,256]{2,1,0:T(8,128)(2,1)}, u32[]{:S(2)}) copy-start(bf16[1,2048,256]{2,1,0:T(8,128)(2,1)} %param.26) | copy-start | bytes 3145732
  7.2 88.2 %all-gather.6.cloned.1.call-start = ((), (), s32[]{:S(2)}) async-start(), calls=%async_computation.4 | async-start | bytes 4456448 | tf_op jit(solution)/shard_map/all_gather | solution.py:110
  53.2 117.2 %all-gather.8.cloned.1.call-start = ((), (), s32[]{:S(2)}) async-start(), calls=%async_computation.5 | async-start | bytes 8912896 | tf_op jit(solution)/shard_map/all_gather | solution.py:122
  99.9 1.3 copy-start.11
  101.2 2.3 copy-start.2
  101.2 2.3 copy-start.3
  101.2 5.5 %copy-start.7 = (f32[31,128]{1,0:T(8,128)S(1)}, f32[31,128]{1,0:T(8,128)}, u32[]{:S(2)}) copy-start(f32[31,128]{1,0:T(8,128)} %param.18) | copy-start | bytes 47620
  101.2 32.4 %copy-start.9 = (f32[128]{0:T(128)S(1)}, f32[128]{0:T(128)}, u32[]{:S(2)}) copy-start(f32[128]{0:T(128)} %param.20) | copy-start | bytes 1540
  101.2 32.4 %copy-start.10 = (f32[128]{0:T(128)S(1)}, f32[128]{0:T(128)}, u32[]{:S(2)}) copy-start(f32[128]{0:T(128)} %param.19) | copy-start | bytes 1540
  103.4 110.9 %all-gather.4.cloned.1.call-start = ((), (), s32[]{:S(2)}) async-start(), calls=%async_computation.3 | async-start | bytes 2228224 | tf_op jit(solution)/shard_map/all_gather | solution.py:81
  103.5 3.9 %collective-permute-start = (bf16[30,128]{1,0:T(8,128)(2,1)S(1)}, bf16[30,128]{1,0:T(8,128)(2,1)S(1)}, u32[]{:S(2)}, u32[]{:S(2)}) collective-permute-start(bf16[30,128]{1,0:T(8,128)(2,1)S(1)} %slice.260), channel_id=1, source_target_pairs={{0,16},{16,32},{32,48},{48,64},{64,80},{80,96},{96,112},{112,128},... | collective-permute-start | bytes 23048 | tf_op jit(solution)/shard_map/ppermute | solution.py:13
  134.6 49.1 %copy-start.4 = (bf16[2048,32]{0,1:T(8,128)(2,1)S(1)}, bf16[2048,32]{0,1:T(8,128)(2,1)}, u32[]{:S(2)}) copy-start(bf16[2048,32]{0,1:T(8,128)(2,1)} %param.29) | copy-start | bytes 393220
  134.6 49.3 %copy-start.8 = (f32[128,4]{0,1:T(4,128)S(1)}, f32[128,4]{0,1:T(4,128)}, u32[]{:S(2)}) copy-start(f32[128,4]{0,1:T(4,128)} %param.25) | copy-start | bytes 6148
  134.6 49.5 %copy-start.5 = (bf16[2048,32]{0,1:T(8,128)(2,1)S(1)}, bf16[2048,32]{0,1:T(8,128)(2,1)}, u32[]{:S(2)}) copy-start(bf16[2048,32]{0,1:T(8,128)(2,1)} %param.30) | copy-start | bytes 393220
  134.6 79.7 %copy-start.1 = (bf16[2048,128]{1,0:T(8,128)(2,1)S(1)}, bf16[2048,128]{1,0:T(8,128)(2,1)}, u32[]{:S(2)}) copy-start(bf16[2048,128]{1,0:T(8,128)(2,1)} %param.21) | copy-start | bytes 1572868
  177.1 41.8 %copy-start.6 = (bf16[512,128]{1,0:T(8,128)(2,1)S(1)}, bf16[512,128]{1,0:T(8,128)(2,1)}, u32[]{:S(2)}) copy-start(bf16[512,128]{1,0:T(8,128)(2,1)} %param.31) | copy-start | bytes 393220
  177.1 23.3 %all-to-all-start.1 = ((bf16[8,4,1,32,128]{4,3,1,2,0:T(8,128)(2,1)}), bf16[8,4,1,32,128]{4,3,1,2,0:T(8,128)(2,1)S(1)}, u32[]{:S(2)}, u32[]{:S(2)}) async-start(bf16[8,4,1,32,128]{4,3,1,2,0:T(8,128)(2,1)} %bitcast.41), calls=%async_computation.1 | async-start | bytes 524288 | tf_op jit(solution)/shard_map/all_to_all | solution.py:31
  201.1 16.1 %all-to-all-start.2 = ((bf16[8,4,1,32,128]{4,3,0,2,1:T(8,128)(2,1)}), bf16[8,4,1,32,128]{4,3,0,2,1:T(8,128)(2,1)S(1)}, u32[]{:S(2)}, u32[]{:S(2)}) async-start(bf16[8,4,1,32,128]{4,3,0,2,1:T(8,128)(2,1)} %copy.39), calls=%async_computation.2 | async-start | bytes 524288 | tf_op jit(solution)/shard_map/all_to_all | solution.py:31
Sparse Core Ops, SparseCore 0:
  53.3 42.0 all-gather.5
  103.5 66.8 all-gather.7
  173.1 41.1 all-gather.3
where the time goes:
time: 227 us; the launch traced here: 226 us
  waiting for transfers between devices  87.8 us (39%)
  blocking collectives  65.9 us (29%)
  local copies, waits for them, and re-layouts  23.3 us (10%)
  matrix products  14.4 us (6%)
  between operations  14 us (6%)
  starting transfers between devices  13.8 us (6%)
  other arithmetic  6.99 us (3%)
    all_gather x1, waiting for transfers between devices, body(): arrived = lax.all_gather(partial_rows, 'tp', axis=1, tiled=True)  42.1 us
    all_gather x1, waiting for transfers between devices, body(): lax.all_gather(expert_hidden, 'tp', axis=1, tiled=True)  35.8 us
    psum x1, blocking collectives, body(): lax.psum((jnp.sum(filtered, axis=1), jnp.sum(filtered * filtered, axis=1)...  25 us
    all_to_all x1, blocking collectives, body(): lax.all_to_all(own_slots, EP, split_axis=0, concat_axis=0, tiled=True)  24.8 us
    all_gather x1, blocking collectives, body(): lax.all_gather(shared_hidden, 'tp', axis=1, tiled=True)  16.1 us
    scatter x1, local copies, waits for them, and re-layouts, body(): outgoing = jnp.zeros((groups * capacity, model_width), jnp.bfloat16).at[s...  12.8 us
    all_to_all x2, starting transfers between devices, exchange_in_order(): lax.all_to_all(parts, axes[k], split_axis=k, concat_axis=k, tiled=True)  10.6 us
    all_gather x1, waiting for transfers between devices, body(): lax.all_gather(conv_hidden, 'tp', axis=1, tiled=True)  9.08 us
  transfers between devices with their start and end apart: 6, of which 4 were waited for; matrix products, arithmetic and copies ran while one was open for 6% of the time, Pallas kernels for 0%

commit v1 on v0

--- a/solution.py
+++ b/solution.py
@@ -5,6 +5,28 @@
 from jax.sharding import PartitionSpec as P
 
 EP = ("ep_0", "ep_1")
+
+
+def joined_along_2(blocks, dim):
+    shape = list(blocks.shape[1:])
+    shape[dim] *= blocks.shape[0]
+    return jnp.moveaxis(blocks, 0, dim).reshape(shape)
+
+
+def gather_around(x, axis, dim):
+    size = lax.axis_size(axis)
+    pairs = [(i, (i + 1) % size) for i in range(size)]
+    back = [(b, a) for a, b in pairs]
+    lower, upper = ([], [])
+    for step in range(size - 1):
+        if step % 2 == 0:
+            lower.append(lax.ppermute(lower[-1] if lower else x, axis, pairs))
+        else:
+            upper.append(lax.ppermute(upper[-1] if upper else x, axis, back))
+    blocks = jnp.stack([*lower[::-1], x, *upper])
+    shift = lax.axis_index(axis) - len(lower)
+    blocks = blocks[(jnp.arange(size) - shift) % size]
+    return joined_along_2(blocks, dim)
 
 
 def from_behind(value, axis, steps):
@@ -124,9 +146,7 @@
         preferred_element_type=jnp.float32,
     )
     shared_sum = jnp.dot(
-        lax.all_gather(shared_hidden, "tp", axis=1, tiled=True),
-        shared_down,
-        preferred_element_type=jnp.float32,
+        gather_around(shared_hidden, "tp", 1), shared_down, preferred_element_type=jnp.float32
     )
     expert_out = routed_sum.astype(jnp.bfloat16).reshape(groups, capacity, columns)
     returned = stepwise_exchange(expert_out, EP, (0, 1), 0, 0).reshape(groups * capacity, columns)

time: 227 us -> 227 us (level)
  starting transfers between devices: 13.8 us -> 36.2 us
  blocking collectives: 65.9 us -> 52.1 us
  waiting for transfers between devices: 87.8 us -> 78.6 us
    all_gather x1, waiting for transfers between devices: 35.8 us -> 7.23 us  [body(): lax.all_gather(expert_hidden, 'tp', axis=1, tiled=True)]
    ppermute x0 -> x15, starting transfers between devices: none -> 22.2 us  [the longest x7 14.1 us: gather_around(): upper.append(lax.ppermute(upper[-1] if upper else x, axis, back))]
    all_gather x1 -> x0, blocking collectives: 16.1 us -> none  [body(): lax.all_gather(shared_hidden, 'tp', axis=1, tiled=True)]
    all_to_all x2, waiting for transfers between devices: 0.01 us -> 11.2 us  [exchange_in_order(): lax.all_to_all(parts, axes[k], split_axis=k, concat_axis=k, tiled=True)]
    all_gather x1, waiting for transfers between devices: 9.08 us -> 14 us  [body(): lax.all_gather(conv_hidden, 'tp', axis=1, tiled=True)]
    ppermute x0 -> x15, waiting for transfers between devices: none -> 3.99 us  [the longest x8 2.39 us: gather_around(): lower.append(lax.ppermute(lower[-1] if lower else x, axis, pairs))]
  transfers between devices with their start and end apart: 6 -> 21, of which waited for: 4 -> 11; matrix products, arithmetic and copies ran while one was open for 6% -> 6% of each run, Pallas kernels for 0% -> 0%
where the time goes in v1:
time: 227 us; the launch traced here: 226 us
  waiting for transfers between devices  78.6 us (35%)
  blocking collectives  52.1 us (23%)
  starting transfers between devices  36.2 us (16%)
  local copies, waits for them, and re-layouts  24.2 us (11%)
  matrix products  14.2 us (6%)
  between operations  14.1 us (6%)
  other arithmetic  6.92 us (3%)
    all_gather x1, waiting for transfers between devices, body(): arrived = lax.all_gather(partial_rows, 'tp', axis=1, tiled=True)  42.1 us
    psum x1, blocking collectives, body(): lax.psum((jnp.sum(filtered, axis=1), jnp.sum(filtered * filtered, axis=1)...  27.3 us
    all_to_all x1, blocking collectives, body(): lax.all_to_all(own_slots, EP, split_axis=0, concat_axis=0, tiled=True)  24.8 us
    ppermute x7, starting transfers between devices, gather_around(): upper.append(lax.ppermute(upper[-1] if upper else x, axis, back))  14.1 us
    all_gather x1, waiting for transfers between devices, body(): lax.all_gather(conv_hidden, 'tp', axis=1, tiled=True)  14 us
    scatter x1, local copies, waits for them, and re-layouts, body(): outgoing = jnp.zeros((groups * capacity, model_width), jnp.bfloat16).at[s...  12.8 us
    all_to_all x2, waiting for transfers between devices, exchange_in_order(): lax.all_to_all(parts, axes[k], split_axis=k, concat_axis=k, tiled=True)  11.2 us
    all_to_all x2, starting transfers between devices, exchange_in_order(): lax.all_to_all(parts, axes[k], split_axis=k, concat_axis=k, tiled=True)  10.7 us
  transfers between devices with their start and end apart: 21, of which 11 were waited for; matrix products, arithmetic and copies ran while one was open for 6% of the time, Pallas kernels for 0%

profile of v1, /device:TPU:1, one launch (start us, length us, event | category | flops | bytes accessed | tf_op | source)
XLA Modules:
  0.0 226.2 jit_solution(13579544581368752729)
XLA Ops:
  13.3 12.8 %scatter_custom_fusion = bf16[1024,2048]{1,0:T(8,128)(2,1)} fusion(s32[512]{0:T(512)S(1)} %bitcast.155, bf16[128,2048]{1,0:T(8,128)(2,1)S(1)} %fusion.8, s32[1024]{0:T(1024)S(1)} %pad_clamp_fusion.2, bf16[]{:T(256)} %constant.63.clone.1), kind=kCustom, calls=%fused_computation.4 | custom fusion | bytes 4194306 | tf_op jit(solution)/shard_map/scatter | solution.py:126
  26.1 1.5 constant_dynamic-slice_fusion
  27.6 24.8 %all_to_all.15 = bf16[32,2,2048]{2,1,0:T(2,128)(2,1)S(1)} all-to-all(bf16[32,2,2048]{2,1,0:T(2,128)(2,1)S(1)} %constant_dynamic-slice_fusion), channel_id=1, replica_groups=mesh['ep_0'=8,'ep_1'=4,'tp'=16] {'ep_0','ep_1'}, dimensions={0} | all-to-all | bytes 524288 | tf_op jit(solution)/shard_map/all_to_all | solution.py:131
  53.3 42.1 %all-gather.6.cloned.1.call-done = bf16[32,32,2048]{2,0,1:T(8,128)(2,1)} async-done(((bf16[32,2,2048]{2,0,1:T(8,128)(2,1)}), bf16[32,32,2048]{2,0,1:T(8,128)(2,1)}) %all-gather.6.cloned.1.call-update) | async-done | bytes 4194320 | tf_op jit(solution)/shard_map/all_gather | solution.py:132
  95.4 4.5 %copy.37 = bf16[32,32,2048]{2,1,0:T(8,128)(2,1)S(1)} copy(bf16[32,32,2048]{2,0,1:T(8,128)(2,1)} %all-gather.6.cloned.1.call-done) | data formatting | bytes 8388608 | tf_op jit(solution)/shard_map/all_gather | solution.py:132
  101.3 2.1 fusion.3
  105.4 3.1 %collective-permute-start = (bf16[30,128]{1,0:T(8,128)(2,1)S(1)}, bf16[30,128]{1,0:T(8,128)(2,1)S(1)}, u32[]{:S(2)}, u32[]{:S(2)}) collective-permute-start(bf16[30,128]{1,0:T(8,128)(2,1)S(1)} %slice.262), channel_id=1, source_target_pairs={{0,16},{16,32},{32,48},{48,64},{64,80},{80,96},{96,112},{112,128},... | collective-permute-start | bytes 23048 | tf_op jit(solution)/shard_map/ppermute | solution.py:35
  108.6 2.0 collective-permute-start.2
  111.5 2.1 collective-permute-start.3
  113.7 1.5 collective-permute-start.10
  116.8 2.8 %collective-permute-start.11 = (bf16[128,32]{0,1:T(8,128)(2,1)S(1)}, bf16[128,32]{0,1:T(8,128)(2,1)S(1)}, u32[]{:S(2)}, u32[]{:S(2)}) collective-permute-start(bf16[128,32]{0,1:T(8,128)(2,1)S(1)} %collective-permute-done.10), channel_id=1, source_target_pairs={{1,0},{2,1},{3,2},{4,3},{5,4},{6,5},{7,6},{8,7},{9,8},{10,9},{11,1... | collective-permute-start | bytes 24584 | tf_op jit(solution)/shard_map/ppermute | solution.py:25
  120.5 3.9 %collective-permute-start.12 = (bf16[128,32]{0,1:T(8,128)(2,1)S(1)}, bf16[128,32]{0,1:T(8,128)(2,1)S(1)}, u32[]{:S(2)}, u32[]{:S(2)}) collective-permute-start(bf16[128,32]{0,1:T(8,128)(2,1)S(1)} %collective-permute-done.11), channel_id=1, source_target_pairs={{1,0},{2,1},{3,2},{4,3},{5,4},{6,5},{7,6},{8,7},{9,8},{10,9},{11,1... | collective-permute-start | bytes 24584 | tf_op jit(solution)/shard_map/ppermute | solution.py:25
  125.9 27.3 %all-reduce = (f32[512]{0:T(512)S(1)}, f32[512]{0:T(512)S(1)}) all-reduce(f32[512]{0:T(512)S(1)} %get-tuple-element.3, f32[512]{0:T(512)S(1)} %get-tuple-element.2), channel_id=1, replica_groups=mesh['ep_0'=8,'ep_1'=4,'tp'=16] {'tp'}, use_global_device_ids=true, to_apply=%region_3.0 | all-reduce | flops 1024 | bytes 8192 | tf_op jit(solution)/shard_map/psum | solution.py:92
  153.2 3.8 %collective-permute-start.13 = (bf16[128,32]{0,1:T(8,128)(2,1)S(1)}, bf16[128,32]{0,1:T(8,128)(2,1)S(1)}, u32[]{:S(2)}, u32[]{:S(2)}) collective-permute-start(bf16[128,32]{0,1:T(8,128)(2,1)S(1)} %collective-permute-done.12), channel_id=1, source_target_pairs={{1,0},{2,1},{3,2},{4,3},{5,4},{6,5},{7,6},{8,7},{9,8},{10,9},{11,1... | collective-permute-start | bytes 24584 | tf_op jit(solution)/shard_map/ppermute | solution.py:25
  158.4 1.8 collective-permute-start.8
  161.6 1.5 collective-permute-start.15
  163.3 7.2 %all-gather.8.cloned.1.call-done = bf16[1024,4096]{1,0:T(8,128)(2,1)} async-done(((bf16[1024,256]{1,0:T(8,128)(2,1)}), bf16[1024,4096]{1,0:T(8,128)(2,1)}) %all-gather.8.cloned.1.call-update) | async-done | bytes 8388624 | tf_op jit(solution)/shard_map/all_gather | solution.py:144
  170.5 6.4 %convolution_convert_fusion = bf16[1024,128]{1,0:T(8,128)(2,1)} fusion(bf16[1024,4096]{1,0:T(8,128)(2,1)} %all-gather.8.cloned.1.call-done, bf16[1,4096,128]{2,1,0:T(8,128)(2,1)S(1)} %copy-done.12), kind=kOutput, calls=%fused_computation.40 | convolution fusion | flops 1073872896 | bytes 9699328 | tf_op jit(solution)/shard_map/dot_general | solution.py:143
  176.9 5.7 %all-to-all-start.1 = ((bf16[8,4,1,32,128]{4,3,1,2,0:T(8,128)(2,1)}), bf16[8,4,1,32,128]{4,3,1,2,0:T(8,128)(2,1)S(1)}, u32[]{:S(2)}, u32[]{:S(2)}) async-start(bf16[8,4,1,32,128]{4,3,1,2,0:T(8,128)(2,1)} %bitcast.41), calls=%async_computation.1 | async-start | bytes 524288 | tf_op jit(solution)/shard_map/all_to_all | solution.py:53
  183.2 11.2 %all-to-all-done.1 = bf16[8,4,1,32,128]{4,3,1,2,0:T(8,128)(2,1)S(1)} async-done(((bf16[8,4,1,32,128]{4,3,1,2,0:T(8,128)(2,1)}), bf16[8,4,1,32,128]{4,3,1,2,0:T(8,128)(2,1)S(1)}, u32[]{:S(2)}, u32[]{:S(2)}) %all-to-all-start.1) | async-done | bytes 262176 | tf_op jit(solution)/shard_map/all_to_all | solution.py:53
  195.1 5.1 %all-to-all-start.2 = ((bf16[8,4,1,32,128]{4,3,0,2,1:T(8,128)(2,1)}), bf16[8,4,1,32,128]{4,3,0,2,1:T(8,128)(2,1)S(1)}, u32[]{:S(2)}, u32[]{:S(2)}) async-start(bf16[8,4,1,32,128]{4,3,0,2,1:T(8,128)(2,1)} %copy.39), calls=%async_computation.2 | async-start | bytes 524288 | tf_op jit(solution)/shard_map/all_to_all | solution.py:53
  200.2 14.0 %all-gather.4.cloned.1.call-done = bf16[512,2048]{1,0:T(8,128)(2,1)} async-done(((bf16[512,128]{1,0:T(8,128)(2,1)}), bf16[512,2048]{1,0:T(8,128)(2,1)}) %all-gather.4.cloned.1.call-update) | async-done | bytes 2097168 | tf_op jit(solution)/shard_map/all_gather | solution.py:103
  214.2 3.0 %convolution_convert_fusion.1 = bf16[512,128]{1,0:T(8,128)(2,1)} fusion(bf16[512,2048]{1,0:T(8,128)(2,1)} %all-gather.4.cloned.1.call-done, bf16[2048,128]{1,0:T(8,128)(2,1)S(1)} %copy-done.1), kind=kOutput, calls=%fused_computation.41 | convolution fusion | flops 268500992 | bytes 2752512 | tf_op jit(solution)/shard_map/dot_general | solution.py:102
  217.2 1.3 gather_fusion
  (110 shorter events, 20.4 us)
Async XLA Ops:
  7.2 92.8 %copy-start = (bf16[1,2048,256]{2,1,0:T(8,128)(2,1)S(1)}, bf16[1,2048,256]{2,1,0:T(8,128)(2,1)}, u32[]{:S(2)}) copy-start(bf16[1,2048,256]{2,1,0:T(8,128)(2,1)} %param.26) | copy-start | bytes 3145732
  7.2 88.3 %all-gather.6.cloned.1.call-start = ((), (), s32[]{:S(2)}) async-start(), calls=%async_computation.4 | async-start | bytes 4456448 | tf_op jit(solution)/shard_map/all_gather | solution.py:132
  53.3 117.3 %all-gather.8.cloned.1.call-start = ((), (), s32[]{:S(2)}) async-start(), calls=%async_computation.5 | async-start | bytes 8912896 | tf_op jit(solution)/shard_map/all_gather | solution.py:144
  101.3 58.9 %copy-start.9 = (f32[128]{0:T(128)S(1)}, f32[128]{0:T(128)}, u32[]{:S(2)}) copy-start(f32[128]{0:T(128)} %param.20) | copy-start | bytes 1540
  101.3 69.2 %copy-start.12 = (bf16[1,4096,128]{2,1,0:T(8,128)(2,1)S(1)}, bf16[1,4096,128]{2,1,0:T(8,128)(2,1)}, u32[]{:S(2)}) copy-start(bf16[1,4096,128]{2,1,0:T(8,128)(2,1)} %param.28) | copy-start | bytes 3145732
  103.5 110.8 %all-gather.4.cloned.1.call-start = ((), (), s32[]{:S(2)}) async-start(), calls=%async_computation.3 | async-start | bytes 2228224 | tf_op jit(solution)/shard_map/all_gather | solution.py:103
  104.1 4.5 %collective-permute-start.1 = (bf16[128,32]{0,1:T(8,128)(2,1)S(1)}, bf16[128,32]{0,1:T(8,128)(2,1)S(1)}, u32[]{:S(2)}, u32[]{:S(2)}) collective-permute-start(bf16[128,32]{0,1:T(8,128)(2,1)S(1)} %fusion.5), channel_id=1, source_target_pairs={{0,1},{1,2},{2,3},{3,4},{4,5},{5,6},{6,7},{7,8},{8,9},{9,10},{10,1... | collective-permute-start | bytes 24584 | tf_op jit(solution)/shard_map/ppermute | solution.py:23
  105.3 8.4 %collective-permute-start.9 = (bf16[128,32]{0,1:T(8,128)(2,1)S(1)}, bf16[128,32]{0,1:T(8,128)(2,1)S(1)}, u32[]{:S(2)}, u32[]{:S(2)}) collective-permute-start(bf16[128,32]{0,1:T(8,128)(2,1)S(1)} %fusion.5), channel_id=1, source_target_pairs={{1,0},{2,1},{3,2},{4,3},{5,4},{6,5},{7,6},{8,7},{9,8},{10,9},{11,1... | collective-permute-start | bytes 24584 | tf_op jit(solution)/shard_map/ppermute | solution.py:25
  105.4 19.3 %collective-permute-start = (bf16[30,128]{1,0:T(8,128)(2,1)S(1)}, bf16[30,128]{1,0:T(8,128)(2,1)S(1)}, u32[]{:S(2)}, u32[]{:S(2)}) collective-permute-start(bf16[30,128]{1,0:T(8,128)(2,1)S(1)} %slice.262), channel_id=1, source_target_pairs={{0,16},{16,32},{32,48},{48,64},{64,80},{80,96},{96,112},{112,128},... | collective-permute-start | bytes 23048 | tf_op jit(solution)/shard_map/ppermute | solution.py:35
  108.6 3.0 %collective-permute-start.2 = (bf16[128,32]{0,1:T(8,128)(2,1)S(1)}, bf16[128,32]{0,1:T(8,128)(2,1)S(1)}, u32[]{:S(2)}, u32[]{:S(2)}) collective-permute-start(bf16[128,32]{0,1:T(8,128)(2,1)S(1)} %collective-permute-done.1), channel_id=1, source_target_pairs={{0,1},{1,2},{2,3},{3,4},{4,5},{5,6},{6,7},{7,8},{8,9},{9,10},{10,1... | collective-permute-start | bytes 24584 | tf_op jit(solution)/shard_map/ppermute | solution.py:23
  111.5 4.3 %collective-permute-start.3 = (bf16[128,32]{0,1:T(8,128)(2,1)S(1)}, bf16[128,32]{0,1:T(8,128)(2,1)S(1)}, u32[]{:S(2)}, u32[]{:S(2)}) collective-permute-start(bf16[128,32]{0,1:T(8,128)(2,1)S(1)} %collective-permute-done.2), channel_id=1, source_target_pairs={{0,1},{1,2},{2,3},{3,4},{4,5},{5,6},{6,7},{7,8},{8,9},{9,10},{10,1... | collective-permute-start | bytes 24584 | tf_op jit(solution)/shard_map/ppermute | solution.py:23
  113.7 3.1 %collective-permute-start.10 = (bf16[128,32]{0,1:T(8,128)(2,1)S(1)}, bf16[128,32]{0,1:T(8,128)(2,1)S(1)}, u32[]{:S(2)}, u32[]{:S(2)}) collective-permute-start(bf16[128,32]{0,1:T(8,128)(2,1)S(1)} %collective-permute-done.9), channel_id=1, source_target_pairs={{1,0},{2,1},{3,2},{4,3},{5,4},{6,5},{7,6},{8,7},{9,8},{10,9},{11,1... | collective-permute-start | bytes 24584 | tf_op jit(solution)/shard_map/ppermute | solution.py:25
  115.8 4.3 %collective-permute-start.4 = (bf16[128,32]{0,1:T(8,128)(2,1)S(1)}, bf16[128,32]{0,1:T(8,128)(2,1)S(1)}, u32[]{:S(2)}, u32[]{:S(2)}) collective-permute-start(bf16[128,32]{0,1:T(8,128)(2,1)S(1)} %collective-permute-done.3), channel_id=1, source_target_pairs={{0,1},{1,2},{2,3},{3,4},{4,5},{5,6},{6,7},{7,8},{8,9},{9,10},{10,1... | collective-permute-start | bytes 24584 | tf_op jit(solution)/shard_map/ppermute | solution.py:23
  116.8 3.8 %collective-permute-start.11 = (bf16[128,32]{0,1:T(8,128)(2,1)S(1)}, bf16[128,32]{0,1:T(8,128)(2,1)S(1)}, u32[]{:S(2)}, u32[]{:S(2)}) collective-permute-start(bf16[128,32]{0,1:T(8,128)(2,1)S(1)} %collective-permute-done.10), channel_id=1, source_target_pairs={{1,0},{2,1},{3,2},{4,3},{5,4},{6,5},{7,6},{8,7},{9,8},{10,9},{11,1... | collective-permute-start | bytes 24584 | tf_op jit(solution)/shard_map/ppermute | solution.py:25
  120.1 4.6 %collective-permute-start.5 = (bf16[128,32]{0,1:T(8,128)(2,1)S(1)}, bf16[128,32]{0,1:T(8,128)(2,1)S(1)}, u32[]{:S(2)}, u32[]{:S(2)}) collective-permute-start(bf16[128,32]{0,1:T(8,128)(2,1)S(1)} %collective-permute-done.4), channel_id=1, source_target_pairs={{0,1},{1,2},{2,3},{3,4},{4,5},{5,6},{6,7},{7,8},{8,9},{9,10},{10,1... | collective-permute-start | bytes 24584 | tf_op jit(solution)/shard_map/ppermute | solution.py:23
  120.5 32.7 %collective-permute-start.12 = (bf16[128,32]{0,1:T(8,128)(2,1)S(1)}, bf16[128,32]{0,1:T(8,128)(2,1)S(1)}, u32[]{:S(2)}, u32[]{:S(2)}) collective-permute-start(bf16[128,32]{0,1:T(8,128)(2,1)S(1)} %collective-permute-done.11), channel_id=1, source_target_pairs={{1,0},{2,1},{3,2},{4,3},{5,4},{6,5},{7,6},{8,7},{9,8},{10,9},{11,1... | collective-permute-start | bytes 24584 | tf_op jit(solution)/shard_map/ppermute | solution.py:25
  124.7 32.3 %collective-permute-start.6 = (bf16[128,32]{0,1:T(8,128)(2,1)S(1)}, bf16[128,32]{0,1:T(8,128)(2,1)S(1)}, u32[]{:S(2)}, u32[]{:S(2)}) collective-permute-start(bf16[128,32]{0,1:T(8,128)(2,1)S(1)} %collective-permute-done.5), channel_id=1, source_target_pairs={{0,1},{1,2},{2,3},{3,4},{4,5},{5,6},{6,7},{7,8},{8,9},{9,10},{10,1... | collective-permute-start | bytes 24584 | tf_op jit(solution)/shard_map/ppermute | solution.py:23
  153.2 4.6 %collective-permute-start.13 = (bf16[128,32]{0,1:T(8,128)(2,1)S(1)}, bf16[128,32]{0,1:T(8,128)(2,1)S(1)}, u32[]{:S(2)}, u32[]{:S(2)}) collective-permute-start(bf16[128,32]{0,1:T(8,128)(2,1)S(1)} %collective-permute-done.12), channel_id=1, source_target_pairs={{1,0},{2,1},{3,2},{4,3},{5,4},{6,5},{7,6},{8,7},{9,8},{10,9},{11,1... | collective-permute-start | bytes 24584 | tf_op jit(solution)/shard_map/ppermute | solution.py:25
  157.0 1.4 collective-permute-start.7
  157.8 3.8 %collective-permute-start.14 = (bf16[128,32]{0,1:T(8,128)(2,1)S(1)}, bf16[128,32]{0,1:T(8,128)(2,1)S(1)}, u32[]{:S(2)}, u32[]{:S(2)}) collective-permute-start(bf16[128,32]{0,1:T(8,128)(2,1)S(1)} %collective-permute-done.13), channel_id=1, source_target_pairs={{1,0},{2,1},{3,2},{4,3},{5,4},{6,5},{7,6},{8,7},{9,8},{10,9},{11,1... | collective-permute-start | bytes 24584 | tf_op jit(solution)/shard_map/ppermute | solution.py:25
  158.4 4.8 %collective-permute-start.8 = (bf16[128,32]{0,1:T(8,128)(2,1)S(1)}, bf16[128,32]{0,1:T(8,128)(2,1)S(1)}, u32[]{:S(2)}, u32[]{:S(2)}) collective-permute-start(bf16[128,32]{0,1:T(8,128)(2,1)S(1)} %collective-permute-done.7), channel_id=1, source_target_pairs={{0,1},{1,2},{2,3},{3,4},{4,5},{5,6},{6,7},{7,8},{8,9},{9,10},{10,1... | collective-permute-start | bytes 24584 | tf_op jit(solution)/shard_map/ppermute | solution.py:23
  161.6 21.0 %collective-permute-start.15 = (bf16[128,32]{0,1:T(8,128)(2,1)S(1)}, bf16[128,32]{0,1:T(8,128)(2,1)S(1)}, u32[]{:S(2)}, u32[]{:S(2)}) collective-permute-start(bf16[128,32]{0,1:T(8,128)(2,1)S(1)} %collective-permute-done.14), channel_id=1, source_target_pairs={{1,0},{2,1},{3,2},{4,3},{5,4},{6,5},{7,6},{8,7},{9,8},{10,9},{11,1... | collective-permute-start | bytes 24584 | tf_op jit(solution)/shard_map/ppermute | solution.py:25
  176.9 17.4 %all-to-all-start.1 = ((bf16[8,4,1,32,128]{4,3,1,2,0:T(8,128)(2,1)}), bf16[8,4,1,32,128]{4,3,1,2,0:T(8,128)(2,1)S(1)}, u32[]{:S(2)}, u32[]{:S(2)}) async-start(bf16[8,4,1,32,128]{4,3,1,2,0:T(8,128)(2,1)} %bitcast.41), calls=%async_computation.1 | async-start | bytes 524288 | tf_op jit(solution)/shard_map/all_to_all | solution.py:53
  195.1 22.1 %all-to-all-start.2 = ((bf16[8,4,1,32,128]{4,3,0,2,1:T(8,128)(2,1)}), bf16[8,4,1,32,128]{4,3,0,2,1:T(8,128)(2,1)S(1)}, u32[]{:S(2)}, u32[]{:S(2)}) async-start(bf16[8,4,1,32,128]{4,3,0,2,1:T(8,128)(2,1)} %copy.39), calls=%async_computation.2 | async-start | bytes 524288 | tf_op jit(solution)/shard_map/all_to_all | solution.py:53
  (10 other events, 192.0 us)
Sparse Core Ops, SparseCore 0:
  53.4 42.0 all-gather.5
  103.6 66.9 all-gather.7
  173.1 41.0 all-gather.3
